TPU v7x, 32 devices: a whole 2x2x4 slice. The times are simulated.
32 devices in a mesh: grp: 2 (over x), ep: 4 (over z), tp: 4 (over y, core).
Axes of the slice: x: 2, y: 2, z: 4, core: 2. Of those that a mesh axis runs over, the one named last changes fastest.
Arguments:
- token_rows: bfloat16 [4096, 2048], P(('grp', 'ep', 'tp')), parts along dimension 0, may hold values from -6 to 6
- norm_gain: float32 [2048], replicated, may hold values from 0.1 to 1.9
- norm_bias: float32 [2048], replicated, may hold values from -3 to 3
- expert_ids: int32 [4096, 2], P(('grp', 'ep', 'tp')), parts along dimension 0, may hold values from 0 to 3, as said below
- route_gates: float32 [4096, 2], P(('grp', 'ep', 'tp')), parts along dimension 0, may hold values from 0.1 to 1
- gate_weight: bfloat16 [4, 2048, 512], P('tp'), may hold values from -0.125 to 0.125
- up_weight: bfloat16 [4, 2048, 512], P('tp'), may hold values from -0.125 to 0.125
- down_weight: bfloat16 [4, 512, 2048], P('tp'), may hold values from -0.25 to 0.25
Outputs:
- combined: bfloat16 [4096, 2048], P(('grp', 'ep', 'tp')), parts along dimension 0
There are 2 independent parts, one for each index of `grp`. A program takes and returns all parts, laid end to end along the dimension named above; an argument that names none is the same for every part. Nothing has to cross between parts.
Inputs may be any that keep to these rules, and one draw needn't show every extreme that they name: `expert_ids`: the two experts of a token are different and lie in one group: both are among 4 * g to 4 * g + 3 for some g. In the rows of one device (aligned blocks of 128 rows) no expert is named more than 64 times, and in every such block each expert of one group is named exactly 64 times; that group is the same for all blocks of a draw.
All inputs are finite; a program needn't handle non-finite values.
Results may differ from a plain program's by a relative error of at most 0.01.
Values may be sent and summed in bfloat16 or wider, within the bound.
A program may use at most 64 MiB of HBM per device.

v0:
```python
import jax
import jax.numpy as jnp
from jax import lax
from jax.sharding import PartitionSpec as P

EPSILON = 1e-05


def layer_norm(token_rows, gain_vec, bias_vec):
    as_float = token_rows.astype(jnp.float32)
    center = jnp.mean(as_float, axis=-1, keepdims=True)
    centered = as_float - center
    variance = jnp.mean(centered * centered, axis=-1, keepdims=True)
    return (centered * lax.rsqrt(variance + EPSILON) * gain_vec + bias_vec).astype(jnp.bfloat16)


def expert_rows(input_rows, gate_matrix, up_matrix, down_matrix, row_gates):
    gate_act = jnp.dot(input_rows, gate_matrix, preferred_element_type=jnp.float32)
    up_act = jnp.dot(input_rows, up_matrix, preferred_element_type=jnp.float32)
    hidden = (jax.nn.silu(gate_act) * up_act).astype(jnp.bfloat16)
    output = jnp.dot(hidden, down_matrix, preferred_element_type=jnp.float32)
    return (row_gates[:, None] * output).astype(jnp.bfloat16)


def rank_within(labels, label_count):
    onehot = (labels[:, None] == jnp.arange(label_count, dtype=jnp.int32)[None, :]).astype(
        jnp.int32
    )
    return jnp.sum((jnp.cumsum(onehot, axis=0) - 1) * onehot, axis=1)


def shards(
    token_rows, norm_gain, norm_bias, expert_ids, route_gates, gate_weight, up_weight, down_weight
):
    tok_count, row_width = token_rows.shape
    tp_count = lax.axis_size("tp")
    capacity = min(4 * tok_count // tp_count, tok_count // 2)
    normed = layer_norm(token_rows, norm_gain, norm_bias)
    zero_row = jnp.zeros((1, row_width), jnp.bfloat16)
    padded = jnp.concatenate([normed, zero_row], axis=0)
    gate_matrix = gate_weight[0]
    up_matrix = up_weight[0]
    down_matrix = down_weight[0]
    flat_ids = expert_ids.reshape(-1)
    target = flat_ids * capacity + rank_within(flat_ids, tp_count)
    owner_row = jnp.arange(2 * tok_count, dtype=jnp.int32) // 2
    row_table = jnp.full((tp_count * capacity,), tok_count, jnp.int32).at[target].set(owner_row)
    gate_table = (
        jnp.zeros((tp_count * capacity,), jnp.float32).at[target].set(route_gates.reshape(-1))
    )
    outgoing = padded[row_table].reshape(tp_count, capacity, row_width)
    out_gates = gate_table.reshape(tp_count, capacity)
    landed = lax.all_to_all(outgoing, "tp", split_axis=0, concat_axis=0, tiled=True)
    landed_gates = lax.all_to_all(
        out_gates.astype(jnp.bfloat16), "tp", split_axis=0, concat_axis=0, tiled=True
    ).astype(out_gates.dtype)
    item_count = landed.shape[1]
    weighted = expert_rows(
        landed.reshape(-1, row_width), gate_matrix, up_matrix, down_matrix, landed_gates.reshape(-1)
    )
    returned = lax.all_to_all(
        weighted.reshape(tp_count, item_count, row_width),
        "tp",
        split_axis=0,
        concat_axis=0,
        tiled=True,
    )
    picked = returned.reshape(tp_count * capacity, row_width)[target]
    picked = picked.reshape(tok_count, 2, row_width).astype(jnp.float32)
    return (picked[:, 0] + picked[:, 1]).astype(jnp.bfloat16)


def solution(mesh):
    placed = (
        P(("grp", "ep", "tp"), None),
        P(),
        P(),
        P(("grp", "ep", "tp"), None),
        P(("grp", "ep", "tp"), None),
        P("tp", None, None),
        P("tp", None, None),
        P("tp", None, None),
    )
    return jax.shard_map(
        shards, mesh=mesh, in_specs=placed, out_specs=P(("grp", "ep", "tp"), None), check_vma=False
    )
```

profile of v0, /device:TPU:0, one launch (start us, length us, event | category | flops | bytes accessed | tf_op | source)
XLA Modules:
  0.0 73.4 jit_solution(8673269340043643683)
XLA Ops:
  0.0 0.8 %broadcast_multiply_fusion = s32[128,2]{0,1:T(2,128)S(1)} fusion(s32[128,2]{0,1:T(2,128)} %param.11), kind=kLoop, calls=%fused_computation.48 | loop fusion | flops 256 | bytes 2048 | tf_op jit(solution)/shard_map/mul | solution.py:45
  0.8 0.8 %copy.22 = s32[128,2]{1,0:T(8,128)S(1)} copy(s32[128,2]{0,1:T(2,128)} %param.11) | data formatting | bytes 2048 | tf_op args[3]
  1.8 0.1 eq.25
  2.0 0.1 mul.55
  2.2 1.2 %reduce-window.6 = s32[4,2,128]{2,1,0:T(2,128)S(1)} reduce-window(s32[4,2,128]{2,1,0:T(2,128)S(1)} %compare_convert_fusion, s32[]{:T(128)} %constant.36.clone.1), window={size=1x1x128 pad=0_0x0_0x127_0}, to_apply=%region_0.0 | reduce-window | flops 130048 | bytes 8196 | tf_op jit(solution)/shard_map/reduce-window
  3.8 0.8 %copy.26 = f32[128,2]{1,0:T(8,128)S(1)} copy(f32[128,2]{0,1:T(2,128)} %param.12) | data formatting | bytes 2048 | tf_op args[4]
  4.8 1.4 %scatter_custom_fusion = f32[256]{0:T(256)S(1)} fusion(s32[256]{0:T(256)S(1)} %bitcast.47, f32[256]{0:T(256)S(1)} %reshape.131, f32[]{:T(128)} %constant.34.clone.1), kind=kCustom, calls=%fused_computation.49 | custom fusion | bytes 1028 | tf_op jit(solution)/shard_map/scatter | solution.py:49
  6.2 0.7 convert_element_type.67
  6.8 4.3 %all-to-all-start = ((bf16[4,1,64]{2,1,0:T(2,128)(2,1)}), bf16[4,1,64]{2,1,0:T(2,128)(2,1)S(1)}, u32[]{:S(2)}, u32[]{:S(2)}) async-start(bf16[4,1,64]{2,1,0:T(2,128)(2,1)} %convert_element_type.67), calls=%async_computation | async-start | bytes 4096 | tf_op jit(solution)/shard_map/all_to_all | solution.py:54
  11.1 1.2 %convert_reduce_fusion = f32[128]{0:T(128)S(1)} fusion(bf16[128,2048]{1,0:T(8,128)(2,1)} %param.8), kind=kLoop, calls=%fused_computation.12 | loop fusion | flops 524160 | bytes 524800 | tf_op jit(solution)/shard_map/reduce_sum | solution.py:11
  12.3 1.3 %fusion.14 = f32[128]{0:T(128)S(1)} fusion(bf16[128,2048]{1,0:T(8,128)(2,1)} %param.8, f32[128]{0:T(128)S(1)} %broadcast_multiply_fusion.1), kind=kLoop, calls=%fused_computation.17 | loop fusion | flops 1048448 | bytes 525312 | tf_op jit(solution)/shard_map/reduce_sum | solution.py:13
  13.6 1.4 %scatter_custom_fusion.1 = s32[256]{0:T(256)S(1)} fusion(s32[256]{0:T(256)S(1)} %bitcast.48, s32[256]{0:T(256)S(1)} %and_select_fusion, s32[]{:T(128)} %constant.42.clone.1), kind=kCustom, calls=%fused_computation.45 | custom fusion | bytes 1028 | tf_op jit(solution)/shard_map/scatter | solution.py:47
  15.1 1.5 %fusion.17 = bf16[128,2048]{1,0:T(8,128)(2,1)S(1)} fusion(bf16[128,2048]{1,0:T(8,128)(2,1)} %param.8, f32[2048]{0:T(1024)} %param.10, f32[2048]{0:T(1024)} %param.9, f32[128]{0:T(128)S(1)} %add_rsqrt_fusion, f32[128]{0:T(128)S(1)} %broadcast_multiply_fusion.1), kind=kLoop, calls=%fused_computation.20 | loop fusion | flops 1572864 | bytes 1065984 | tf_op jit(solution)/shard_map/convert_element_type | solution.py:14
  16.6 2.3 %gather_fusion = bf16[256,2048]{1,0:T(8,128)(2,1)} fusion(bf16[129,2048]{1,0:T(8,128)(2,1)S(1)} %concatenate.3, s32[1024]{0:T(1024)S(1)} %pad_clamp_fusion.1), kind=kCustom, calls=%fused_computation | custom fusion | bytes 2098176 | tf_op jit(solution)/shard_map/gather | solution.py:51
  18.9 3.5 %all-to-all-start.1 = ((bf16[4,64,2048]{2,1,0:T(8,128)(2,1)}), bf16[4,64,2048]{2,1,0:T(8,128)(2,1)S(1)}, u32[]{:S(2)}, u32[]{:S(2)}) async-start(bf16[4,64,2048]{2,1,0:T(8,128)(2,1)} %bitcast.43), calls=%async_computation.1 | async-start | bytes 2097152 | tf_op jit(solution)/shard_map/all_to_all | solution.py:53
  22.6 14.3 %all-to-all-done.1 = bf16[4,64,2048]{2,1,0:T(8,128)(2,1)S(1)} async-done(((bf16[4,64,2048]{2,1,0:T(8,128)(2,1)}), bf16[4,64,2048]{2,1,0:T(8,128)(2,1)S(1)}, u32[]{:S(2)}, u32[]{:S(2)}) %all-to-all-start.1) | async-done | bytes 1048608 | tf_op jit(solution)/shard_map/all_to_all | solution.py:53
  36.9 3.1 %fusion.4 = f32[256,512]{1,0:T(8,128)} fusion(bf16[256,2048]{1,0:T(8,128)(2,1)S(1)} %bitcast.44, bf16[1,2048,512]{2,1,0:T(8,128)(2,1)} %param.13), kind=kOutput, calls=%fused_computation.9 | convolution fusion | flops 536870912 | bytes 3670016 | tf_op jit(solution)/shard_map/dot_general | solution.py:18
  40.0 4.0 %fusion = bf16[256,2048]{1,0:T(8,128)(2,1)} fusion(bf16[1,512,2048]{2,1,0:T(8,128)(2,1)S(1)} %copy-done, f32[256]{0:T(256)S(1)} %reshape.109, bf16[256,2048]{1,0:T(8,128)(2,1)S(1)} %bitcast.45, bf16[1,2048,512]{2,1,0:T(8,128)(2,1)} %param.14, f32[256,512]{1,0:T(8,128)} %fusion.4), kind=kOutput, calls=%fused_computation.5 | convolution fusion | flops 1075576832 | bytes 6816768 | tf_op jit(solution)/shard_map/dot_general | solution.py:21
  44.0 3.5 %all-to-all-start.2 = ((bf16[4,64,2048]{2,1,0:T(8,128)(2,1)}), bf16[4,64,2048]{2,1,0:T(8,128)(2,1)S(1)}, u32[]{:S(2)}, u32[]{:S(2)}) async-start(bf16[4,64,2048]{2,1,0:T(8,128)(2,1)} %bitcast.46), calls=%async_computation.2 | async-start | bytes 2097152 | tf_op jit(solution)/shard_map/all_to_all | solution.py:61
  47.5 14.4 %all-to-all-done.2 = bf16[4,64,2048]{2,1,0:T(8,128)(2,1)S(1)} async-done(((bf16[4,64,2048]{2,1,0:T(8,128)(2,1)}), bf16[4,64,2048]{2,1,0:T(8,128)(2,1)S(1)}, u32[]{:S(2)}, u32[]{:S(2)}) %all-to-all-start.2) | async-done | bytes 1048608 | tf_op jit(solution)/shard_map/all_to_all | solution.py:61
  61.9 2.3 %gather_fusion.1 = bf16[256,2048]{1,0:T(8,128)(2,1)} fusion(bf16[256,2048]{1,0:T(8,128)(2,1)S(1)} %bitcast.42, s32[1024]{0:T(1024)S(1)} %pad_clamp_fusion), kind=kCustom, calls=%fused_computation.1 | custom fusion | bytes 2098176 | tf_op jit(solution)/shard_map/gather | solution.py:68
  64.2 3.4 %reshape.110 = f32[128,2,2048]{2,1,0:T(2,128)} reshape(bf16[256,2048]{1,0:T(8,128)(2,1)} %gather_fusion.1) | data formatting | bytes 3145728 | tf_op jit(solution)/shard_map/convert_element_type | solution.py:69
  67.6 4.4 %fusion.35 = (f32[128,1,2048]{2,1,0:T(1,128)S(1)}, f32[128,1,2048]{2,1,0:T(1,128)S(1)}) fusion(f32[128,2,2048]{2,1,0:T(2,128)} %reshape.110), kind=kLoop, calls=%fused_computation.53 | loop fusion | bytes 4194304 | tf_op jit(solution)/shard_map/slice | solution.py:70
  72.0 1.4 %fusion.21 = bf16[128,2048]{1,0:T(8,128)(2,1)} fusion(f32[128,1,2048]{2,1,0:T(1,128)S(1)} %get-tuple-element.6, f32[128,1,2048]{2,1,0:T(1,128)S(1)} %get-tuple-element.5), kind=kLoop, calls=%fused_computation.23 | loop fusion | flops 524288 | bytes 2621440 | tf_op jit(solution)/shard_map/convert_element_type | solution.py:70
  (25 shorter events, 1.0 us)
Async XLA Ops:
  0.0 40.0 %copy-start = (bf16[1,512,2048]{2,1,0:T(8,128)(2,1)S(1)}, bf16[1,512,2048]{2,1,0:T(8,128)(2,1)}, u32[]{:S(2)}) copy-start(bf16[1,512,2048]{2,1,0:T(8,128)(2,1)} %param.15) | copy-start | bytes 6291460
  6.8 12.1 %all-to-all-start = ((bf16[4,1,64]{2,1,0:T(2,128)(2,1)}), bf16[4,1,64]{2,1,0:T(2,128)(2,1)S(1)}, u32[]{:S(2)}, u32[]{:S(2)}) async-start(bf16[4,1,64]{2,1,0:T(2,128)(2,1)} %convert_element_type.67), calls=%async_computation | async-start | bytes 4096 | tf_op jit(solution)/shard_map/all_to_all | solution.py:54
  18.9 17.9 %all-to-all-start.1 = ((bf16[4,64,2048]{2,1,0:T(8,128)(2,1)}), bf16[4,64,2048]{2,1,0:T(8,128)(2,1)S(1)}, u32[]{:S(2)}, u32[]{:S(2)}) async-start(bf16[4,64,2048]{2,1,0:T(8,128)(2,1)} %bitcast.43), calls=%async_computation.1 | async-start | bytes 2097152 | tf_op jit(solution)/shard_map/all_to_all | solution.py:53
  44.0 17.9 %all-to-all-start.2 = ((bf16[4,64,2048]{2,1,0:T(8,128)(2,1)}), bf16[4,64,2048]{2,1,0:T(8,128)(2,1)S(1)}, u32[]{:S(2)}, u32[]{:S(2)}) async-start(bf16[4,64,2048]{2,1,0:T(8,128)(2,1)} %bitcast.46), calls=%async_computation.2 | async-start | bytes 2097152 | tf_op jit(solution)/shard_map/all_to_all | solution.py:61
where the time goes:
time: 73.9 us; the launch traced here: 73.4 us
  waiting for transfers between devices  28.7 us (39%)
  local copies, waits for them, and re-layouts  18.6 us (25%)
  starting transfers between devices  11.3 us (15%)
  other arithmetic  7.61 us (10%)
  matrix products  7.1 us (10%)
    all_to_all x1, waiting for transfers between devices, shards(): lax.all_to_all(weighted.reshape(tp_count, item_count, row_width), 'tp', s...  14.4 us
    all_to_all x1, waiting for transfers between devices, shards(): lax.all_to_all(outgoing, 'tp', split_axis=0, concat_axis=0, tiled=True)  14.3 us
    slice x1, local copies, waits for them, and re-layouts, shards(): return (picked[:, 0] + picked[:, 1]).astype(jnp.bfloat16)  4.37 us
    all_to_all x1, starting transfers between devices, shards(): lax.all_to_all(out_gates.astype(jnp.bfloat16), 'tp', split_axis=0, concat...  4.26 us
    dot_general x1, matrix products, expert_rows(): output = jnp.dot(hidden, down_matrix, preferred_element_type=jnp.float32)  4.01 us
    all_to_all x1, starting transfers between devices, shards(): lax.all_to_all(outgoing, 'tp', split_axis=0, concat_axis=0, tiled=True)  3.52 us
    all_to_all x1, starting transfers between devices, shards(): lax.all_to_all(weighted.reshape(tp_count, item_count, row_width), 'tp', s...  3.51 us
    convert_element_type x1, local copies, waits for them, and re-layouts, shards(): picked = picked.reshape(tok_count, 2, row_width).astype(jnp.float32)  3.39 us
  transfers between devices with their start and end apart: 3, of which 2 were waited for; matrix products, arithmetic and copies ran while one was open for 11% of the time, Pallas kernels for 0%

commit v1 on v0

v1 whole, which is shorter than its diff:
```python
import functools

import jax
import jax.numpy as jnp
from jax import lax
from jax.experimental import pallas as pl
from jax.experimental.pallas import tpu as pltpu
from jax.sharding import PartitionSpec as P

EPSILON = 1e-05
F32 = jnp.float32
BF16 = jnp.bfloat16
MESH = pl.DeviceIdType.MESH
CHUNK_ROWS = 32
NORM_ROWS = 16


def dot(a, b):
    return jnp.dot(a, b, preferred_element_type=F32)


def kernel(
    tp_count, cores, capacity, chunks,
    tokens_ref, gain_ref, bias_ref, ids_ref, gates_ref, wg_hbm, wu_hbm, wd_hbm,
    out_ref,
    wg, wu, wd, normed, near_out, near_in, near_res, near_back, far_out, far_in, far_res, far_back, total,
    w_sem, near_send, near_recv, near_rsend, near_rrecv, far_send, far_recv, far_rsend, far_rrecv,
):
    tok_count, width = tokens_ref.shape
    chips = tp_count // cores
    far = tp_count - cores
    rows = capacity // chunks
    me = lax.axis_index("tp")
    my_chip, my_core = me // cores, me % cores

    def peer(slot):
        return (my_chip + slot // cores) % chips * cores + (my_core + slot % cores) % cores

    def origin(slot):
        return (my_chip + chips - slot // cores) % chips * cores + (my_core + cores - slot % cores) % cores

    loads = [
        pltpu.make_async_copy(src.at[0], dst, w_sem.at[i])
        for i, (src, dst) in enumerate(((wg_hbm, wg), (wu_hbm, wu), (wd_hbm, wd)))
    ]
    for load in loads:
        load.start()
    barrier = pltpu.get_barrier_semaphore()
    for slot in range(1, tp_count):
        pl.semaphore_signal(barrier, inc=1, device_id={"tp": peer(slot)}, device_id_type=MESH)

    gain = gain_ref[...]
    bias = bias_ref[...]

    def norm_block(i, carry):
        at = pl.ds(pl.multiple_of(i * NORM_ROWS, NORM_ROWS), NORM_ROWS)
        x = tokens_ref[at, :].astype(F32)
        center = jnp.mean(x, axis=-1, keepdims=True)
        centered = x - center
        variance = jnp.mean(centered * centered, axis=-1, keepdims=True)
        normed[at, :] = (centered * lax.rsqrt(variance + EPSILON) * gain + bias).astype(BF16)
        return carry

    lax.fori_loop(0, tok_count // NORM_ROWS, norm_block, 0, unroll=2)

    ids = ids_ref[...]
    gates = gates_ref[...]
    lanes = 128 * pl.cdiv(tp_count, 128)
    lane = lax.broadcasted_iota(jnp.int32, (tok_count, lanes), 1)
    first = ids[:, 0:1] == lane
    second = ids[:, 1:2] == lane
    named = jnp.where(first | second, 1.0, 0.0)
    gate_of = jnp.where(first, gates[:, 0:1], 0.0) + jnp.where(second, gates[:, 1:2], 0.0)
    t_row = lax.broadcasted_iota(jnp.int32, (tok_count, tok_count), 0)
    t_col = lax.broadcasted_iota(jnp.int32, (tok_count, tok_count), 1)
    before = jnp.where(t_col < t_row, 1.0, 0.0).astype(BF16)
    rank = dot(before, named.astype(BF16))
    place = jnp.where(named > 0.5, rank, -1.0)
    place_t = place.T

    expert_of_row = lax.broadcasted_iota(jnp.int32, (lanes, tok_count), 0)

    def place_row(slot):
        return jnp.sum(jnp.where(expert_of_row == peer(slot), place_t, 0.0), axis=0, keepdims=True).astype(jnp.int32)

    def pick(slot, start, count):
        want = start + lax.broadcasted_iota(jnp.int32, (count, tok_count), 0)
        return jnp.where(place_row(slot) == want, 1.0, 0.0).astype(BF16)

    def far_copy(c, f):
        return pltpu.make_async_remote_copy(
            far_out.at[c, f], far_in.at[c, f], far_send.at[c, f], far_recv.at[c, f],
            device_id={"tp": peer(cores + f)}, device_id_type=MESH)

    def far_return(c, f):
        return pltpu.make_async_remote_copy(
            far_res.at[c, f], far_back.at[c, f], far_rsend.at[c, f], far_rrecv.at[c, f],
            device_id={"tp": origin(cores + f)}, device_id_type=MESH)

    def near_copy(s):
        return pltpu.make_async_remote_copy(
            near_out.at[s], near_in.at[s], near_send.at[s], near_recv.at[s],
            device_id={"tp": peer(s)}, device_id_type=MESH)

    def near_return(s):
        return pltpu.make_async_remote_copy(
            near_res.at[s], near_back.at[s], near_rsend.at[s], near_rrecv.at[s],
            device_id={"tp": origin(s)}, device_id_type=MESH)

    for c in range(chunks):
        picks = jnp.concatenate([pick(cores + f, c * rows, rows) for f in range(far)], axis=0)
        far_out[c] = dot(picks, normed[...]).astype(BF16).reshape(far, rows, width)
        if c == 0:
            pl.semaphore_wait(barrier, tp_count - 1)
        for f in range(far):
            far_copy(c, f).start()
    near_picks = jnp.concatenate([pick(s, 0, capacity) for s in range(cores)], axis=0)
    packed = dot(near_picks, normed[...]).astype(BF16).reshape(cores, capacity, width)
    near_in[0] = packed[0]
    for s in range(1, cores):
        near_out[s] = packed[s]
        near_copy(s).start()

    def expert(rows_in):
        gate_act = dot(rows_in, wg[...])
        up_act = dot(rows_in, wu[...])
        hidden = (gate_act / (1.0 + jnp.exp(-gate_act)) * up_act).astype(BF16)
        return dot(hidden, wd[...]).astype(BF16)

    for load in loads:
        load.wait()
    for s in range(1, cores):
        near_copy(s).wait_recv()
    results = expert(near_in[...].reshape(cores * capacity, width)).reshape(cores, capacity, width)
    near_back[0] = results[0]
    for s in range(1, cores):
        near_res[s] = results[s]
        near_return(s).start()

    def far_step(c, carry):
        for f in range(far):
            far_copy(c, f).wait_recv()
        done = expert(far_in[c].reshape(far * rows, width)).reshape(far, rows, width)
        far_res[c] = done
        for f in range(far):
            far_return(c, f).start()
        return carry

    lax.fori_loop(0, chunks, far_step, 0)

    def spread(slots, start, count):
        want = lax.broadcasted_iota(jnp.int32, (tok_count, len(slots) * count), 1)
        high = jnp.zeros(want.shape, F32)
        for i, slot in enumerate(slots):
            mine = lane == peer(slot)
            at = jnp.sum(jnp.where(mine, place, 0.0), axis=1, keepdims=True).astype(jnp.int32) - start
            gate = jnp.sum(jnp.where(mine, gate_of, 0.0), axis=1, keepdims=True)
            at = jnp.where((at >= 0) & (at < count), at + i * count, -1)
            high = high + jnp.where(at == want, gate, 0.0)
        coarse = high.astype(BF16)
        return coarse, (high - coarse.astype(F32)).astype(BF16)

    for s in range(1, cores):
        near_return(s).wait_recv()
    coarse, fine = spread(range(cores), 0, capacity)
    back = near_back[...].reshape(cores * capacity, width)
    total[...] = dot(coarse, back) + dot(fine, back)

    for c in range(chunks):
        coarse, fine = spread(range(cores, tp_count), c * rows, rows)
        for f in range(far):
            far_return(c, f).wait_recv()
        back = far_back[c].reshape(far * rows, width)
        part = total[...] + (dot(coarse, back) + dot(fine, back))
        if c + 1 < chunks:
            total[...] = part
        else:
            out_ref[...] = part.astype(BF16)
    for s in range(1, cores):
        near_copy(s).wait_send()
        near_return(s).wait_send()

    def drain(c, carry):
        for f in range(far):
            far_copy(c, f).wait_send()
            far_return(c, f).wait_send()
        return carry

    lax.fori_loop(0, chunks, drain, 0)


def shards(token_rows, norm_gain, norm_bias, expert_ids, route_gates, gate_weight, up_weight, down_weight):
    tok_count, width = token_rows.shape
    hidden = gate_weight.shape[2]
    tp_count = lax.axis_size("tp")
    capacity = min(4 * tok_count // tp_count, tok_count // 2)
    cores = 2
    far = tp_count - cores
    chunks = max(1, capacity // CHUNK_ROWS)
    rows = capacity // chunks
    vmem = pl.BlockSpec(memory_space=pltpu.VMEM)
    hbm = pl.BlockSpec(memory_space=pl.ANY)
    near = pltpu.VMEM((cores, capacity, width), BF16)
    distant = pltpu.VMEM((chunks, far, rows, width), BF16)
    near_sem = pltpu.SemaphoreType.DMA((cores,))
    far_sem = pltpu.SemaphoreType.DMA((chunks, far))
    return pl.pallas_call(
        functools.partial(kernel, tp_count, cores, capacity, chunks),
        out_shape=jax.ShapeDtypeStruct((tok_count, width), BF16),
        in_specs=[vmem] * 5 + [hbm] * 3,
        out_specs=vmem,
        scratch_shapes=[
            pltpu.VMEM((width, hidden), BF16),
            pltpu.VMEM((width, hidden), BF16),
            pltpu.VMEM((hidden, width), BF16),
            pltpu.VMEM((tok_count, width), BF16),
            near, near, near, near,
            distant, distant, distant, distant,
            pltpu.VMEM((tok_count, width), F32),
            pltpu.SemaphoreType.DMA((3,)),
            near_sem, near_sem, near_sem, near_sem,
            far_sem, far_sem, far_sem, far_sem,
        ],
        compiler_params=pltpu.CompilerParams(
            collective_id=0, has_side_effects=True, vmem_limit_bytes=60 * 1024 * 1024
        ),
    )(
        token_rows, norm_gain.reshape(1, width), norm_bias.reshape(1, width),
        expert_ids, route_gates, gate_weight, up_weight, down_weight,
    )


def solution(mesh):
    rows = P(("grp", "ep", "tp"), None)
    weight = P("tp", None, None)
    return jax.shard_map(
        shards, mesh=mesh,
        in_specs=(rows, P(), P(), rows, rows, weight, weight, weight),
        out_specs=rows, check_vma=False,
    )
```

time: 73.9 us -> 34.4 us (0.47)
  Pallas kernels: 0 us -> 29.3 us
  waiting for transfers between devices: 28.7 us -> 0 us
  local copies, waits for them, and re-layouts: 18.6 us -> 4.7 us
  starting transfers between devices: 11.3 us -> 0 us
  other arithmetic: 7.61 us -> 0 us
  matrix products: 7.1 us -> 0 us
    pallas_call x0 -> x1, Pallas kernels: none -> 29.3 us  [shards(): pl.pallas_call(functools.partial(kernel, tp_count, cores, capacity, chunk...]
    all_to_all x3 -> x0, waiting for transfers between devices: 28.7 us -> none  [the longest x1 14.4 us: shards(): lax.all_to_all(weighted.reshape(tp_count, item_count, row_width), 'tp', s...]
    all_to_all x3 -> x0, starting transfers between devices: 11.3 us -> none  [the longest x1 4.26 us: shards(): lax.all_to_all(out_gates.astype(jnp.bfloat16), 'tp', split_axis=0, concat...]
    dot_general x2 -> x0, matrix products: 7.1 us -> none  [the longest x1 4.01 us: expert_rows(): output = jnp.dot(hidden, down_matrix, preferred_element_type=jnp.float32)]
    gather x2 -> x0, local copies, waits for them, and re-layouts: 4.69 us -> none  [the longest x1 2.35 us: shards(): outgoing = padded[row_table].reshape(tp_count, capacity, row_width)]
    slice x3 -> x0, local copies, waits for them, and re-layouts: 4.55 us -> none  [the longest x1 4.37 us: shards(): return (picked[:, 0] + picked[:, 1]).astype(jnp.bfloat16)]
    convert_element_type x3 -> x0, local copies, waits for them, and re-layouts: 4.14 us -> none  [the longest x1 3.39 us: shards(): picked = picked.reshape(tok_count, 2, row_width).astype(jnp.float32)]
    unnamed x4 -> x3, local copies, waits for them, and re-layouts: 1.58 us -> 4.7 us
  transfers between devices with their start and end apart: 3 -> 0, of which waited for: 2 -> 0; matrix products, arithmetic and copies ran while one was open for 11% -> 0% of each run, Pallas kernels for 0% -> 0%
where the time goes in v1:
time: 34.4 us; the launch traced here: 34.1 us
  Pallas kernels  29.3 us (85%)
  local copies, waits for them, and re-layouts  4.7 us (14%)
    pallas_call x1, Pallas kernels, shards(): pl.pallas_call(functools.partial(kernel, tp_count, cores, capacity, chunk...  29.3 us
    unnamed x3, local copies, waits for them, and re-layouts  4.7 us

profile of v1, /device:TPU:0, one launch (start us, length us, event | category | flops | bytes accessed | tf_op | source)
XLA Modules:
  0.0 34.1 jit_solution(5215902237951385622)
XLA Ops:
  0.0 1.4 %copy.9.ids_ref = s32[128,2]{1,0:T(8,128)} copy(s32[128,2]{0,1:T(2,128)} %param.11) | data formatting | bytes 2048 | tf_op args[3]
  1.4 1.4 %copy.10.gates_ref = f32[128,2]{1,0:T(8,128)} copy(f32[128,2]{0,1:T(2,128)} %param.12) | data formatting | bytes 2048 | tf_op args[4]
  2.8 29.3 %shard_map.82 = bf16[128,2048]{1,0:T(8,128)(2,1)} custom-call(bf16[128,2048]{1,0:T(8,128)(2,1)} %tokens_ref.1, f32[1,2048]{1,0:T(1,128)} %bitcast.2, f32[1,2048]{1,0:T(1,128)} %bitcast.3, s32[128,2]{1,0:T(8,128)} %copy.9.ids_ref, f32[128,2]{1,0:T(8,128)} %copy.10.gates_ref, bf16[1,2048,512]{2,1,0:T(8,128)(2,1)} %wg_hbm.1, bf16[1,2048,512]{2,1,0:T(8,128)(2,1)} %wu_hbm.1, ...), custom_call_target="tpu_custom_call" | custom-call | tf_op jit(solution)/shard_map/pallas_call | solution.py:207
  32.2 1.9 %copy.12 = bf16[128,2048]{1,0:T(8,128)(2,1)} copy(bf16[128,2048]{1,0:T(8,128)(2,1)} %shard_map.82) | data formatting | bytes 1048576

commit v2 on v1

v2 whole, which is shorter than its diff:
```python
import functools

import jax
import jax.numpy as jnp
from jax import lax
from jax.experimental import pallas as pl
from jax.experimental.pallas import tpu as pltpu
from jax.sharding import PartitionSpec as P

EPSILON = 1e-05
F32 = jnp.float32
BF16 = jnp.bfloat16
MESH = pl.DeviceIdType.MESH
CHUNK_ROWS = 32
NORM_ROWS = 16
BLOCKS = 4
VMEM_BYTES = 60 * 1024 * 1024
IN_SPACE = pltpu.HBM


def dot(a, b):
    return jnp.dot(a, b, preferred_element_type=F32)


def kernel(
    tp_count, cores, capacity, chunks,
    tokens_hbm, gain_hbm, bias_hbm, ids_hbm, gates_hbm, wg_hbm, wu_hbm, wd_hbm,
    out_hbm,
    tokens, gain_ref, bias_ref, ids_ref, gates_ref, wg, wu, wd, normed,
    near_out, near_in, near_res, near_back, far_out, far_in, far_res, far_back, total, result,
    w_sem, out_sem, near_send, near_recv, near_rsend, near_rrecv, far_send, far_recv, far_rsend, far_rrecv,
):
    tok_count, width = tokens.shape
    chips = tp_count // cores
    far = tp_count - cores
    rows = capacity // chunks
    block = width // BLOCKS
    me = lax.axis_index("tp")
    my_chip, my_core = me // cores, me % cores

    def peer(slot):
        return (my_chip + slot // cores) % chips * cores + (my_core + slot % cores) % cores

    def origin(slot):
        return (my_chip + chips - slot // cores) % chips * cores + (my_core + cores - slot % cores) % cores

    barrier = pltpu.get_barrier_semaphore()
    for slot in range(1, tp_count):
        pl.semaphore_signal(barrier, inc=1, device_id={"tp": peer(slot)}, device_id_type=MESH)
    pairs = (
        (ids_hbm, ids_ref), (tokens_hbm, tokens), (gates_hbm, gates_ref), (gain_hbm, gain_ref), (bias_hbm, bias_ref),
        (wg_hbm.at[0], wg), (wu_hbm.at[0], wu), (wd_hbm.at[0], wd),
    )
    loads = [pltpu.make_async_copy(src, dst, w_sem.at[i]) for i, (src, dst) in enumerate(pairs)]
    for load in loads:
        load.start()

    lanes = 128 * pl.cdiv(tp_count, 128)
    t_row = lax.broadcasted_iota(jnp.int32, (tok_count, tok_count), 0)
    t_col = lax.broadcasted_iota(jnp.int32, (tok_count, tok_count), 1)
    before = jnp.where(t_row < t_col, 1.0, 0.0).astype(BF16)
    expert_of_row = lax.broadcasted_iota(jnp.int32, (lanes, tok_count), 0)
    loads[0].wait()
    ids = ids_ref[...]
    first = ids[0:1, :] == expert_of_row
    second = ids[1:2, :] == expert_of_row
    named = jnp.where(first | second, 1.0, 0.0)
    rank = dot(named.astype(BF16), before)
    place_t = jnp.where(named > 0.5, rank, -1.0)

    def place_row(slot):
        return jnp.sum(jnp.where(expert_of_row == peer(slot), place_t, 0.0), axis=0, keepdims=True).astype(jnp.int32)

    def pick(slot, start, count):
        want = start + lax.broadcasted_iota(jnp.int32, (count, tok_count), 0)
        return jnp.where(place_row(slot) == want, 1.0, 0.0).astype(BF16)

    def far_copy(c, f):
        return pltpu.make_async_remote_copy(
            far_out.at[c, f], far_in.at[c, f], far_send.at[c, f], far_recv.at[c, f],
            device_id={"tp": peer(cores + f)}, device_id_type=MESH)

    def far_return(c, f, j):
        at = pl.ds(j * block, block)
        return pltpu.make_async_remote_copy(
            far_res.at[c, f, :, at], far_back.at[c, f, :, at], far_rsend.at[c, f, j], far_rrecv.at[c, f, j],
            device_id={"tp": origin(cores + f)}, device_id_type=MESH)

    def near_copy(s):
        return pltpu.make_async_remote_copy(
            near_out.at[s], near_in.at[s], near_send.at[s], near_recv.at[s],
            device_id={"tp": peer(s)}, device_id_type=MESH)

    def near_return(s):
        return pltpu.make_async_remote_copy(
            near_res.at[s], near_back.at[s], near_rsend.at[s], near_rrecv.at[s],
            device_id={"tp": origin(s)}, device_id_type=MESH)

    for c in range(chunks):
        picks = jnp.concatenate([pick(cores + f, c * rows, rows) for f in range(far)], axis=0)
        if c == 0:
            loads[1].wait()
        far_out[c] = dot(picks, tokens[...]).astype(BF16).reshape(far, rows, width)
        if c == 0:
            pl.semaphore_wait(barrier, tp_count - 1)
        for f in range(far):
            far_copy(c, f).start()
    near_picks = jnp.concatenate([pick(s, 0, capacity) for s in range(cores)], axis=0)
    packed = dot(near_picks, tokens[...]).astype(BF16).reshape(cores, capacity, width)
    near_in[0] = packed[0]
    for s in range(1, cores):
        near_out[s] = packed[s]
        near_copy(s).start()

    for load in loads[2:5]:
        load.wait()
    gates = gates_ref[...]
    place = place_t.T
    gate_of = (jnp.where(first, gates[0:1, :], 0.0) + jnp.where(second, gates[1:2, :], 0.0)).T
    lane = lax.broadcasted_iota(jnp.int32, (tok_count, lanes), 1)

    def norm(load_rows, count):
        gain = gain_ref[...]
        bias = bias_ref[...]

        def norm_block(i, carry):
            at = pl.multiple_of(i * NORM_ROWS, NORM_ROWS)
            x = load_rows(at).astype(F32)
            center = jnp.mean(x, axis=-1, keepdims=True)
            centered = x - center
            variance = jnp.mean(centered * centered, axis=-1, keepdims=True)
            normed[pl.ds(at, NORM_ROWS), :] = (centered * lax.rsqrt(variance + EPSILON) * gain + bias).astype(BF16)
            return carry

        lax.fori_loop(0, count // NORM_ROWS, norm_block, 0)

    def hidden_of(count):
        rows_in = normed[pl.ds(0, count), :]
        gate_act = dot(rows_in, wg[...])
        up_act = dot(rows_in, wu[...])
        return (gate_act / (1.0 + jnp.exp(-gate_act)) * up_act).astype(BF16)

    for s in range(1, cores):
        near_copy(s).wait_recv()
    norm(lambda at: near_in[at // capacity, pl.ds(pl.multiple_of(at % capacity, NORM_ROWS), NORM_ROWS), :], cores * capacity)
    for load in loads[5:]:
        load.wait()
    results = dot(hidden_of(cores * capacity), wd[...]).astype(BF16).reshape(cores, capacity, width)
    near_back[0] = results[0]
    for s in range(1, cores):
        near_res[s] = results[s]
        near_return(s).start()

    def far_step(c, carry):
        for f in range(far):
            far_copy(c, f).wait_recv()
        norm(lambda at: far_in[c, at // rows, pl.ds(pl.multiple_of(at % rows, NORM_ROWS), NORM_ROWS), :], far * rows)
        hidden = hidden_of(far * rows)
        for j in range(BLOCKS):
            at = pl.ds(j * block, block)
            far_res[c, :, :, at] = dot(hidden, wd[:, at]).astype(BF16).reshape(far, rows, block)
            for f in range(far):
                far_return(c, f, j).start()
        return carry

    lax.fori_loop(0, chunks, far_step, 0)

    def spread(slots, start, count):
        want = lax.broadcasted_iota(jnp.int32, (tok_count, len(slots) * count), 1)
        high = jnp.zeros(want.shape, F32)
        for i, slot in enumerate(slots):
            mine = lane == peer(slot)
            at = jnp.sum(jnp.where(mine, place, 0.0), axis=1, keepdims=True).astype(jnp.int32) - start
            gate = jnp.sum(jnp.where(mine, gate_of, 0.0), axis=1, keepdims=True)
            at = jnp.where((at >= 0) & (at < count), at + i * count, -1)
            high = high + jnp.where(at == want, gate, 0.0)
        coarse = high.astype(BF16)
        return coarse, (high - coarse.astype(F32)).astype(BF16)

    for s in range(1, cores):
        near_return(s).wait_recv()
    coarse, fine = spread(range(cores), 0, capacity)
    back = near_back[...].reshape(cores * capacity, width)
    total[...] = dot(coarse, back) + dot(fine, back)

    for c in range(chunks):
        coarse, fine = spread(range(cores, tp_count), c * rows, rows)
        for j in range(BLOCKS):
            at = pl.ds(j * block, block)
            for f in range(far):
                far_return(c, f, j).wait_recv()
            back = far_back[c, :, :, at].reshape(far * rows, block)
            part = total[:, at] + (dot(coarse, back) + dot(fine, back))
            if c + 1 < chunks:
                total[:, at] = part
            else:
                result[:, at] = part.astype(BF16)
                pltpu.make_async_copy(result.at[:, at], out_hbm.at[:, at], out_sem.at[j]).start()
    for s in range(1, cores):
        near_copy(s).wait_send()
        near_return(s).wait_send()

    def drain(c, carry):
        for f in range(far):
            far_copy(c, f).wait_send()
            for j in range(BLOCKS):
                far_return(c, f, j).wait_send()
        return carry

    lax.fori_loop(0, chunks, drain, 0)
    for j in range(BLOCKS):
        at = pl.ds(j * block, block)
        pltpu.make_async_copy(result.at[:, at], out_hbm.at[:, at], out_sem.at[j]).wait()


def shards(token_rows, norm_gain, norm_bias, expert_ids, route_gates, gate_weight, up_weight, down_weight):
    tok_count, width = token_rows.shape
    hidden = gate_weight.shape[2]
    tp_count = lax.axis_size("tp")
    capacity = min(4 * tok_count // tp_count, tok_count // 2)
    cores = 2
    far = tp_count - cores
    chunks = max(1, capacity // CHUNK_ROWS)
    rows = capacity // chunks
    near = pltpu.VMEM((cores, capacity, width), BF16)
    distant = pltpu.VMEM((chunks, far, rows, width), BF16)
    near_sem = pltpu.SemaphoreType.DMA((cores,))
    far_sem = pltpu.SemaphoreType.DMA((chunks, far))
    ret_sem = pltpu.SemaphoreType.DMA((chunks, far, BLOCKS))
    return pl.pallas_call(
        functools.partial(kernel, tp_count, cores, capacity, chunks),
        out_shape=jax.ShapeDtypeStruct((tok_count, width), BF16),
        in_specs=[pl.BlockSpec(memory_space=IN_SPACE)] * 8,
        out_specs=pl.BlockSpec(memory_space=pl.ANY),
        scratch_shapes=[
            pltpu.VMEM((tok_count, width), BF16),
            pltpu.VMEM((1, width), F32),
            pltpu.VMEM((1, width), F32),
            pltpu.VMEM((2, tok_count), jnp.int32),
            pltpu.VMEM((2, tok_count), F32),
            pltpu.VMEM((width, hidden), BF16),
            pltpu.VMEM((width, hidden), BF16),
            pltpu.VMEM((hidden, width), BF16),
            pltpu.VMEM((max(cores * capacity, far * rows), width), BF16),
            near, near, near, near,
            distant, distant, distant, distant,
            pltpu.VMEM((tok_count, width), F32),
            pltpu.VMEM((tok_count, width), BF16),
            pltpu.SemaphoreType.DMA((8,)),
            pltpu.SemaphoreType.DMA((BLOCKS,)),
            near_sem, near_sem, near_sem, near_sem,
            far_sem, far_sem, ret_sem, ret_sem,
        ],
        compiler_params=pltpu.CompilerParams(
            collective_id=0, has_side_effects=True, vmem_limit_bytes=VMEM_BYTES
        ),
    )(
        token_rows, norm_gain.reshape(1, width), norm_bias.reshape(1, width),
        expert_ids.T, route_gates.T, gate_weight, up_weight, down_weight,
    )


def solution(mesh):
    rows = P(("grp", "ep", "tp"), None)
    weight = P("tp", None, None)
    return jax.shard_map(
        shards, mesh=mesh,
        in_specs=(rows, P(), P(), rows, rows, weight, weight, weight),
        out_specs=rows, check_vma=False,
    )
```

time: 34.4 us -> 30.5 us (0.89)
  local copies, waits for them, and re-layouts: 4.7 us -> 1.88 us
  Pallas kernels: 29.3 us -> 28.5 us
    unnamed x3 -> x1, local copies, waits for them, and re-layouts: 4.7 us -> 1.88 us
    pallas_call x1, Pallas kernels: 29.3 us -> 28.5 us  [shards(): pl.pallas_call(functools.partial(kernel, tp_count, cores, capacity, chunk...]
where the time goes in v2:
time: 30.5 us; the launch traced here: 30.4 us
  Pallas kernels  28.5 us (93%)
  local copies, waits for them, and re-layouts  1.88 us (6%)
    pallas_call x1, Pallas kernels, shards(): pl.pallas_call(functools.partial(kernel, tp_count, cores, capacity, chunk...  28.5 us
    unnamed x1, local copies, waits for them, and re-layouts  1.88 us

profile of v2, /device:TPU:0, one launch (start us, length us, event | category | flops | bytes accessed | tf_op | source)
XLA Modules:
  0.0 30.4 jit_solution(2795634550794394572)
XLA Ops:
  0.0 28.5 %shard_map.82 = bf16[128,2048]{1,0:T(8,128)(2,1)} custom-call(bf16[128,2048]{1,0:T(8,128)(2,1)} %tokens_hbm.1, f32[1,2048]{1,0:T(1,128)} %bitcast.4, f32[1,2048]{1,0:T(1,128)} %bitcast.5, s32[2,128]{1,0:T(2,128)} %bitcast.6, f32[2,128]{1,0:T(2,128)} %bitcast.7, bf16[1,2048,512]{2,1,0:T(8,128)(2,1)} %wg_hbm.1, bf16[1,2048,512]{2,1,0:T(8,128)(2,1)} %wu_hbm.1, ...), custom_call_target="tpu_custom_call" | custom-call | tf_op jit(solution)/shard_map/pallas_call | solution.py:230
  28.5 1.9 %copy.10 = bf16[128,2048]{1,0:T(8,128)(2,1)} copy(bf16[128,2048]{1,0:T(8,128)(2,1)} %shard_map.82) | data formatting | bytes 1048576

commit v3 on v2

--- a/solution.py
+++ b/solution.py
@@ -13,8 +13,8 @@
 MESH = pl.DeviceIdType.MESH
 CHUNK_ROWS = 32
 NORM_ROWS = 16
-BLOCKS = 4
-VMEM_BYTES = 60 * 1024 * 1024
+BLOCKS = 2
+VMEM_BYTES = 48 * 1024 * 1024
 IN_SPACE = pltpu.HBM
 
 
@@ -25,10 +25,10 @@
 def kernel(
     tp_count, cores, capacity, chunks,
     tokens_hbm, gain_hbm, bias_hbm, ids_hbm, gates_hbm, wg_hbm, wu_hbm, wd_hbm,
-    out_hbm,
+    out_ref,
     tokens, gain_ref, bias_ref, ids_ref, gates_ref, wg, wu, wd, normed,
-    near_out, near_in, near_res, near_back, far_out, far_in, far_res, far_back, total, result,
-    w_sem, out_sem, near_send, near_recv, near_rsend, near_rrecv, far_send, far_recv, far_rsend, far_rrecv,
+    near_out, near_in, near_res, near_back, far_out, far_in, far_res, far_back, total,
+    w_sem, near_send, near_recv, near_rsend, near_rrecv, far_send, far_recv, far_rsend, far_rrecv,
 ):
     tok_count, width = tokens.shape
     chips = tp_count // cores
@@ -194,8 +194,7 @@
             if c + 1 < chunks:
                 total[:, at] = part
             else:
-                result[:, at] = part.astype(BF16)
-                pltpu.make_async_copy(result.at[:, at], out_hbm.at[:, at], out_sem.at[j]).start()
+                out_ref[:, at] = part.astype(BF16)
     for s in range(1, cores):
         near_copy(s).wait_send()
         near_return(s).wait_send()
@@ -208,9 +207,6 @@
         return carry
 
     lax.fori_loop(0, chunks, drain, 0)
-    for j in range(BLOCKS):
-        at = pl.ds(j * block, block)
-        pltpu.make_async_copy(result.at[:, at], out_hbm.at[:, at], out_sem.at[j]).wait()
 
 
 def shards(token_rows, norm_gain, norm_bias, expert_ids, route_gates, gate_weight, up_weight, down_weight):
@@ -229,9 +225,9 @@
     ret_sem = pltpu.SemaphoreType.DMA((chunks, far, BLOCKS))
     return pl.pallas_call(
         functools.partial(kernel, tp_count, cores, capacity, chunks),
-        out_shape=jax.ShapeDtypeStruct((tok_count, width), BF16),
+        out_shape=pltpu.VMEM((tok_count, width), BF16),
         in_specs=[pl.BlockSpec(memory_space=IN_SPACE)] * 8,
-        out_specs=pl.BlockSpec(memory_space=pl.ANY),
+        out_specs=pl.BlockSpec(memory_space=pltpu.VMEM),
         scratch_shapes=[
             pltpu.VMEM((tok_count, width), BF16),
             pltpu.VMEM((1, width), F32),
@@ -245,9 +241,7 @@
             near, near, near, near,
             distant, distant, distant, distant,
             pltpu.VMEM((tok_count, width), F32),
-            pltpu.VMEM((tok_count, width), BF16),
             pltpu.SemaphoreType.DMA((8,)),
-            pltpu.SemaphoreType.DMA((BLOCKS,)),
             near_sem, near_sem, near_sem, near_sem,
             far_sem, far_sem, ret_sem, ret_sem,
         ],
@@ -255,8 +249,10 @@
             collective_id=0, has_side_effects=True, vmem_limit_bytes=VMEM_BYTES
         ),
     )(
-        token_rows, norm_gain.reshape(1, width), norm_bias.reshape(1, width),
-        expert_ids.T, route_gates.T, gate_weight, up_weight, down_weight,
+        *(pltpu.with_memory_space_constraint(x, pltpu.HBM) for x in (
+            token_rows, norm_gain.reshape(1, width), norm_bias.reshape(1, width),
+            expert_ids.T, route_gates.T, gate_weight, up_weight, down_weight,
+        ))
     )
 
 

time: 30.5 us -> 28.4 us (0.931)
  Pallas kernels: 28.5 us -> 27.4 us
  local copies, waits for them, and re-layouts: 1.88 us -> 0.8 us
    pallas_call x1, Pallas kernels: 28.5 us -> 27.4 us  [shards(): pl.pallas_call(functools.partial(kernel, tp_count, cores, capacity, chunk...]
    unnamed x1, local copies, waits for them, and re-layouts: 1.88 us -> 0.8 us
where the time goes in v3:
time: 28.4 us; the launch traced here: 28.2 us
  Pallas kernels  27.4 us (96%)
  local copies, waits for them, and re-layouts  0.8 us (3%)
    pallas_call x1, Pallas kernels, shards(): pl.pallas_call(functools.partial(kernel, tp_count, cores, capacity, chunk...  27.4 us
    unnamed x1, local copies, waits for them, and re-layouts  0.8 us

profile of v3, /device:TPU:0, one launch (start us, length us, event | category | flops | bytes accessed | tf_op | source)
XLA Modules:
  0.0 28.2 jit_solution(12721482333054691374)
XLA Ops:
  0.0 27.4 %shard_map.82 = bf16[128,2048]{1,0:T(8,128)(2,1)S(1)} custom-call(bf16[128,2048]{1,0:T(8,128)(2,1)} %tokens_hbm.1, f32[1,2048]{1,0:T(1,128)} %bitcast.4, f32[1,2048]{1,0:T(1,128)} %bitcast.5, s32[2,128]{1,0:T(2,128)} %bitcast.6, f32[2,128]{1,0:T(2,128)} %bitcast.7, bf16[1,2048,512]{2,1,0:T(8,128)(2,1)} %wg_hbm.1, bf16[1,2048,512]{2,1,0:T(8,128)(2,1)} %wu_hbm.1, ...), custom_call_target="tpu_custom_call" | custom-call | tf_op jit(solution)/shard_map/pallas_call | solution.py:226
  27.4 0.8 %copy.10 = bf16[128,2048]{1,0:T(8,128)(2,1)} copy(bf16[128,2048]{1,0:T(8,128)(2,1)S(1)} %shard_map.82) | data formatting | bytes 1048576

commit v4 on v3

--- a/solution.py
+++ b/solution.py
@@ -13,7 +13,7 @@
 MESH = pl.DeviceIdType.MESH
 CHUNK_ROWS = 32
 NORM_ROWS = 16
-BLOCKS = 2
+BLOCKS = 1
 VMEM_BYTES = 48 * 1024 * 1024
 IN_SPACE = pltpu.HBM
 
@@ -175,22 +175,22 @@
             at = jnp.where((at >= 0) & (at < count), at + i * count, -1)
             high = high + jnp.where(at == want, gate, 0.0)
         coarse = high.astype(BF16)
-        return coarse, (high - coarse.astype(F32)).astype(BF16)
+        return jnp.concatenate([coarse, (high - coarse.astype(F32)).astype(BF16)], axis=1)
 
     for s in range(1, cores):
         near_return(s).wait_recv()
-    coarse, fine = spread(range(cores), 0, capacity)
+    weights = spread(range(cores), 0, capacity)
     back = near_back[...].reshape(cores * capacity, width)
-    total[...] = dot(coarse, back) + dot(fine, back)
+    total[...] = dot(weights, jnp.concatenate([back, back], axis=0))
 
     for c in range(chunks):
-        coarse, fine = spread(range(cores, tp_count), c * rows, rows)
+        weights = spread(range(cores, tp_count), c * rows, rows)
         for j in range(BLOCKS):
             at = pl.ds(j * block, block)
             for f in range(far):
                 far_return(c, f, j).wait_recv()
             back = far_back[c, :, :, at].reshape(far * rows, block)
-            part = total[:, at] + (dot(coarse, back) + dot(fine, back))
+            part = total[:, at] + dot(weights, jnp.concatenate([back, back], axis=0))
             if c + 1 < chunks:
                 total[:, at] = part
             else:

time: 28.4 us -> 28.3 us (level)
  no operation moved by 1% of the time
where the time goes in v4:
time: 28.3 us; the launch traced here: 28 us
  Pallas kernels  27.2 us (96%)
  local copies, waits for them, and re-layouts  0.8 us (3%)
    pallas_call x1, Pallas kernels, shards(): pl.pallas_call(functools.partial(kernel, tp_count, cores, capacity, chunk...  27.2 us
    unnamed x1, local copies, waits for them, and re-layouts  0.8 us

profile of v4, /device:TPU:0, one launch (start us, length us, event | category | flops | bytes accessed | tf_op | source)
XLA Modules:
  0.0 28.0 jit_solution(16260328686249244330)
XLA Ops:
  0.0 27.2 %shard_map.82 = bf16[128,2048]{1,0:T(8,128)(2,1)S(1)} custom-call(bf16[128,2048]{1,0:T(8,128)(2,1)} %tokens_hbm.1, f32[1,2048]{1,0:T(1,128)} %bitcast.4, f32[1,2048]{1,0:T(1,128)} %bitcast.5, s32[2,128]{1,0:T(2,128)} %bitcast.6, f32[2,128]{1,0:T(2,128)} %bitcast.7, bf16[1,2048,512]{2,1,0:T(8,128)(2,1)} %wg_hbm.1, bf16[1,2048,512]{2,1,0:T(8,128)(2,1)} %wu_hbm.1, ...), custom_call_target="tpu_custom_call" | custom-call | tf_op jit(solution)/shard_map/pallas_call | solution.py:226
  27.2 0.8 %copy.10 = bf16[128,2048]{1,0:T(8,128)(2,1)} copy(bf16[128,2048]{1,0:T(8,128)(2,1)S(1)} %shard_map.82) | data formatting | bytes 1048576
